TPU v7x, 32 devices: a whole 2x2x4 slice. The times are simulated.
32 devices in a mesh: sp: 8 (over z, x), tp: 4 (over y, core).
Axes of the slice: x: 2, y: 2, z: 4, core: 2. Of those that a mesh axis runs over, the one named last changes fastest.
Arguments:
- resid: bfloat16 [2048, 4096], P('sp'), may hold values from -6 to 6
- pool_in: bfloat16 [2048, 1024], P('sp', 'tp'), may hold values from -6 to 6
- pool_mix: bfloat16 [4, 256, 256], P('tp'), may hold values from -0.375 to 0.375
- pool_gain: float32 [1024], P('tp'), may hold values from 0.1 to 1.9
- out_proj: bfloat16 [1024, 4096], P('tp'), may hold values from -0.1875 to 0.1875
- norm_gain: float32 [4096], replicated, may hold values from 0.1 to 1.9
- w_gate: bfloat16 [8, 4096, 1024], P('sp', None, 'tp'), may hold values from -0.09375 to 0.09375
- w_up: bfloat16 [8, 4096, 1024], P('sp', None, 'tp'), may hold values from -0.09375 to 0.09375
- w_down: bfloat16 [8, 1024, 4096], P('sp', 'tp'), may hold values from -0.1875 to 0.1875
- routes: int32 [2048, 2], P('sp'), may hold values from 0 to 7, all different within a row; in each aligned block of 64 rows (0 to 63, 64 to 127, ...) at most 32 rows name the same one
- route_weight: float32 [2048, 2], P('sp'), may hold values from 0.25 to 2.5
Outputs:
- layer_out: bfloat16 [2048, 4096], P(('sp', 'tp'))
Inputs may be any that keep to these rules, and one draw needn't show every extreme that they name: `routes`: in each aligned block of 64 tokens no expert is named by more than 32 of the block's rows, and the two experts of a token differ.
All inputs are finite; a program needn't handle non-finite values.
Results may differ from a plain program's by a relative error of at most 0.015.
Values may be sent and summed in bfloat16 or wider, within the bound.
A program may use at most 128 MiB of HBM per device.

v0:
```python
import jax
import jax.numpy as jnp
from jax import lax
from jax.sharding import PartitionSpec as P

GROUPS = 4


EPS = 1e-06


def shifted(x, axis, by):
    count = lax.axis_size(axis)
    pairs = [(i, i + by) for i in range(count) if 0 <= i + by < count]
    return lax.ppermute(x, axis, pairs)


def rounded(value):
    return lax.optimization_barrier(value.astype(jnp.bfloat16)).astype(jnp.float32)


def group_diff(pool_in):
    row_count = pool_in.shape[0]
    reach = 2**GROUPS
    before = shifted(pool_in[row_count - reach :], "sp", 1)
    joined = jnp.concatenate([before, pool_in], axis=0).astype(jnp.float32)
    running = jnp.cumsum(joined, axis=0)
    width = jnp.left_shift(jnp.int32(2), lax.axis_index("tp"))
    lagged = lax.dynamic_slice_in_dim(running, reach - width, row_count, 0)
    total = running[reach:] - lagged
    place = lax.axis_index("sp") * row_count + jnp.arange(row_count, dtype=jnp.int32) + 1
    counted = jnp.minimum(place, width).astype(jnp.float32)
    return (total / counted[:, None] - joined[reach:]).astype(jnp.bfloat16)


def normalize(mixed, norm_gain):
    scale = lax.rsqrt(jnp.mean(mixed * mixed, axis=1, keepdims=True) + EPS)
    return (mixed * scale * norm_gain).astype(jnp.bfloat16)


def slot_plan(route_rows, blocks, capacity, experts):
    row_count, choose = route_rows.shape
    flat_routes = route_rows.reshape(blocks, row_count // blocks * choose)
    onehot = (
        flat_routes[:, :, None] == jnp.arange(experts, dtype=jnp.int32)[None, None, :]
    ).astype(jnp.int32)
    earlier = jnp.cumsum(onehot, axis=1) - onehot
    position = jnp.sum(earlier * onehot, axis=2)
    block_ids = jnp.arange(blocks, dtype=jnp.int32)[:, None]
    return (flat_routes * (blocks * capacity) + block_ids * capacity + position).reshape(-1)


def fill_slots(normed, targets, slot_count):
    row_count, width = normed.shape
    choose = targets.shape[0] // row_count
    sources = jnp.arange(row_count * choose, dtype=jnp.int32) // choose
    owner = jnp.full((slot_count,), row_count, jnp.int32).at[targets].set(sources)
    extended = jnp.concatenate([normed, jnp.zeros((1, width), normed.dtype)], axis=0)
    return extended[owner]


def collect(returned, targets, weights):
    row_count, choose = weights.shape
    picked = returned[targets]
    weighted = picked * weights.reshape(-1, 1)
    return jnp.sum(weighted.reshape(row_count, choose, -1), axis=1)


def expert_part(inputs, w_gate, w_up, w_down):
    gate = jnp.dot(inputs, w_gate[0], preferred_element_type=jnp.float32)
    upper = jnp.dot(inputs, w_up[0], preferred_element_type=jnp.float32)
    hidden = (jax.nn.silu(gate) * upper).astype(jnp.bfloat16)
    return jnp.dot(hidden, w_down[0], preferred_element_type=jnp.float32).astype(jnp.bfloat16)


def on_device(
    resid,
    pool_in,
    pool_mix,
    pool_gain,
    out_proj,
    norm_gain,
    w_gate,
    w_up,
    w_down,
    routes,
    route_weight,
):
    token_count, width = resid.shape
    choose = routes.shape[1]
    experts = lax.axis_size("sp")
    slices = lax.axis_size("tp")
    sub_count = token_count // slices
    capacity = max(2, 2 * sub_count * choose // experts)
    tp_index = lax.axis_index("tp")
    diff = group_diff(pool_in)
    pooled = (jnp.dot(diff, pool_mix[0], preferred_element_type=jnp.float32) * pool_gain).astype(
        jnp.bfloat16
    )
    proj = rounded(
        lax.psum_scatter(
            rounded(jnp.dot(pooled, out_proj, preferred_element_type=jnp.float32)).astype(
                jnp.bfloat16
            ),
            "tp",
            scatter_dimension=0,
            tiled=True,
        ).astype(jnp.float32)
    )
    first = tp_index * sub_count
    mixed = lax.dynamic_slice_in_dim(resid, first, sub_count, 0).astype(jnp.float32) + proj
    normed = normalize(mixed, norm_gain)
    route_rows = lax.dynamic_slice_in_dim(routes, first, sub_count, 0)
    weight_rows = lax.dynamic_slice_in_dim(route_weight, first, sub_count, 0)
    targets = slot_plan(route_rows, 1, capacity, experts)
    outgoing = fill_slots(normed, targets, experts * capacity).reshape(experts, capacity, width)
    arrived = lax.all_to_all(outgoing, "sp", split_axis=0, concat_axis=0, tiled=True)
    block_rows = lax.all_gather(arrived, "tp", axis=0, tiled=True)
    spread = expert_part(block_rows.reshape(-1, width), w_gate, w_up, w_down).reshape(
        block_rows.shape
    )
    stacked = spread.reshape((slices,) + arrived.shape)
    received = lax.all_to_all(stacked, "tp", split_axis=0, concat_axis=0, tiled=True)
    summed = jnp.sum(received.astype(jnp.float32), axis=0)
    returned = lax.all_to_all(
        summed.astype(jnp.bfloat16), "sp", split_axis=0, concat_axis=0, tiled=True
    ).astype(summed.dtype)
    moe = collect(returned.reshape(-1, width), targets, weight_rows)
    return (mixed + moe).astype(jnp.bfloat16)


def solution(mesh):
    in_specs = (
        P("sp", None),
        P("sp", "tp"),
        P("tp", None, None),
        P("tp"),
        P("tp", None),
        P(),
        P("sp", None, "tp"),
        P("sp", None, "tp"),
        P("sp", "tp", None),
        P("sp", None),
        P("sp", None),
    )
    out_specs = P(("sp", "tp"), None)
    return jax.shard_map(
        on_device, mesh=mesh, in_specs=in_specs, out_specs=out_specs, check_vma=False
    )
```

profile of v0, /device:TPU:8, one launch (start us, length us, event | category | flops | bytes accessed | tf_op | source)
XLA Modules:
  0.0 361.5 jit_solution(666184547438477695)
XLA Ops:
  6.5 0.0 reduce-scatter.2.cloned.1.call-start
  6.5 0.8 slice.19
  7.4 3.4 collective-permute-start
  10.8 3.0 collective-permute-done
  13.8 0.9 fusion.24
  14.8 0.0 copy-start.2
  14.8 0.0 copy-start.4
  14.8 0.3 fusion.12
  15.2 0.1 broadcast_add_fusion
  15.3 0.1 copy.22
  15.4 0.3 copy-done.2
  15.7 0.0 copy-done.4
  15.7 3.8 %convolution_convert_fusion.1 = bf16[256,4096]{1,0:T(8,128)(2,1)} fusion(bf16[256,4096]{1,0:T(8,128)(2,1)} %param.15, f32[272,256]{1,0:T(8,128)S(1)} %get-tuple-element.8, f32[384,256]{1,0:T(8,128)S(1)} %bitcast.45, f32[272,256]{1,0:T(8,128)S(1)} %slice.32, s32[]{:T(128)S(6)} %select_n.28, bf16[1,256,256]{2,1,0:T(8,128)(2,1)S(1)} %copy-done.2, ...), kind=kOutput, calls=%fused_computation.4 | convolution fusion | flops 571867136 | bytes 5113860 | tf_op jit(solution)/shard_map/dot_general | solution.py:102
  19.5 0.0 reduce-scatter.2.cloned.1.call-update
  19.5 0.0 all-gather.2.cloned.1.call-start
  19.6 0.6 copy-done.5
  20.2 0.1 broadcast_multiply_fusion
  20.3 0.1 copy.24
  20.4 0.1 eq.27
  20.5 0.1 fusion.23
  20.6 0.2 reduce_window_sum.28
  20.8 0.1 copy.23
  20.9 0.1 mul.82
  21.0 0.2 select_reduce_fusion
  21.2 1.0 scatter_custom_fusion
  22.2 28.9 %reduce-scatter.2.cloned.1.call-done = bf16[64,4096]{1,0:T(8,128)(2,1)} async-done(((bf16[256,4096]{1,0:T(8,128)(2,1)}), bf16[64,4096]{1,0:T(8,128)(2,1)}) %reduce-scatter.2.cloned.1.call-update) | async-done | bytes 524304 | tf_op jit(solution)/shard_map/reduce_scatter | solution.py:101
  51.1 1.5 multiply_reduce_fusion.1
  52.6 1.4 multiply_convert_fusion
  54.1 3.2 gather_fusion
  57.3 53.3 %all_to_all.15 = bf16[8,32,4096]{2,1,0:T(8,128)(2,1)} all-to-all(bf16[8,32,4096]{2,1,0:T(8,128)(2,1)} %bitcast.43), channel_id=1, replica_groups=mesh['sp'=8,'tp'=4] {'sp'}, dimensions={0} | all-to-all | bytes 4194304 | tf_op jit(solution)/shard_map/all_to_all | solution.py:117
  110.6 0.0 all-gather.2.cloned.1.call-update
  110.6 56.9 %all-gather.2.cloned.1.call-done = bf16[32,32,4096]{2,1,0:T(8,128)(2,1)} async-done(((bf16[8,32,4096]{2,1,0:T(8,128)(2,1)}), bf16[32,32,4096]{2,1,0:T(8,128)(2,1)}) %all-gather.2.cloned.1.call-update) | async-done | bytes 8388624 | tf_op jit(solution)/shard_map/all_gather | solution.py:118
  167.5 6.5 %fusion.3 = f32[1024,256]{1,0:T(8,128)S(1)} fusion(bf16[1024,4096]{1,0:T(8,128)(2,1)} %bitcast.48, bf16[1,4096,256]{2,1,0:T(8,128)(2,1)} %param.17), kind=kOutput, calls=%fused_computation.9 | convolution fusion | flops 2147483648 | bytes 11534336 | tf_op jit(solution)/shard_map/dot_general | solution.py:70
  174.0 0.5 copy-done.8
  174.5 2.4 fusion.8
  176.8 2.4 convolution_convert_fusion
  179.2 96.9 %all_to_all.16 = bf16[4,8,32,4096]{3,2,1,0:T(8,128)(2,1)} all-to-all(bf16[4,8,32,4096]{3,2,1,0:T(8,128)(2,1)S(1)} %bitcast.42), channel_id=1, replica_groups=mesh['sp'=8,'tp'=4] {'tp'}, dimensions={0} | all-to-all | bytes 16777216 | tf_op jit(solution)/shard_map/all_to_all | solution.py:123
  276.1 7.0 %reduce_sum.44 = bf16[8,32,4096]{2,1,0:T(8,128)(2,1)} reduce(bf16[4,8,32,4096]{3,2,1,0:T(8,128)(2,1)} %all_to_all.16, bf16[]{:T(256)} %constant.60.clone.1), dimensions={0}, to_apply=%region_7.8 | reduce | flops 3145728 | bytes 10485762 | tf_op jit(solution)/shard_map/reduce_sum | solution.py:124
  283.0 6.2 %all-to-all-start.2 = ((bf16[8,32,4096]{2,1,0:T(8,128)(2,1)}), bf16[8,32,4096]{2,1,0:T(8,128)(2,1)}, u32[]{:S(2)}, u32[]{:S(2)}) async-start(bf16[8,32,4096]{2,1,0:T(8,128)(2,1)} %reduce_sum.44), calls=%async_computation.3 | async-start | bytes 4194304 | tf_op jit(solution)/shard_map/all_to_all | solution.py:125
  289.2 0.1 constant_dynamic-slice_fusion
  289.3 0.1 copy.25
  289.4 45.2 %all-to-all-done.2 = bf16[8,32,4096]{2,1,0:T(8,128)(2,1)} async-done(((bf16[8,32,4096]{2,1,0:T(8,128)(2,1)}), bf16[8,32,4096]{2,1,0:T(8,128)(2,1)}, u32[]{:S(2)}, u32[]{:S(2)}) %all-to-all-start.2) | async-done | bytes 2097184 | tf_op jit(solution)/shard_map/all_to_all | solution.py:125
  334.6 4.0 %bitcast_convert_fusion = f32[256,4096]{1,0:T(8,128)} fusion(bf16[8,32,4096]{2,1,0:T(8,128)(2,1)} %all-to-all-done.2), kind=kLoop, calls=%fused_computation.5 | loop fusion | flops 1048576 | bytes 6291456 | tf_op jit(solution)/shard_map/reshape | solution.py:128
  338.6 5.6 %gather_fusion.1 = f32[128,4096]{1,0:T(8,128)} fusion(f32[256,4096]{1,0:T(8,128)} %bitcast_convert_fusion, s32[1024]{0:T(1024)S(1)} %pad_clamp_fusion), kind=kCustom, calls=%fused_computation.1 | custom fusion | bytes 4194816 | tf_op jit(solution)/shard_map/gather | solution.py:64
  344.3 3.5 gather.10
  347.8 4.8 %multiply_reduce_fusion = f32[64,4096]{1,0:T(8,128)S(1)} fusion(f32[64,2,4096]{2,1,0:T(2,128)} %gather.10, f32[64,2]{1,0:T(8,128)S(1)} %copy.25), kind=kLoop, calls=%fused_computation.11 | loop fusion | flops 786432 | bytes 3146240 | tf_op jit(solution)/shard_map/reduce_sum | solution.py:66
  352.6 0.0 copy-done.1
  352.6 2.0 add_convert_fusion
  (23 shorter events, 0.2 us)
Async XLA Ops:
  6.5 170.3 %copy-start = (bf16[1,256,4096]{2,1,0:T(8,128)(2,1)S(1)}, bf16[1,256,4096]{2,1,0:T(8,128)(2,1)}, u32[]{:S(2)}) copy-start(bf16[1,256,4096]{2,1,0:T(8,128)(2,1)} %param.19) | copy-start | bytes 6291460
  6.5 44.6 %reduce-scatter.2.cloned.1.call-start = ((), (), s32[]{:S(2)}) async-start(), calls=%async_computation.4 | async-start | bytes 2621440 | tf_op jit(solution)/shard_map/reduce_scatter | solution.py:101
  7.4 6.4 %collective-permute-start = (bf16[16,256]{1,0:T(8,128)(2,1)S(1)}, bf16[16,256]{1,0:T(8,128)(2,1)S(1)}, u32[]{:S(2)}, u32[]{:S(2)}) collective-permute-start(bf16[16,256]{1,0:T(8,128)(2,1)S(1)} %slice.19), channel_id=1, source_target_pairs={{0,4},{4,8},{8,12},{12,16},{16,20},{20,24},{24,28},{1,5},{5,9},{9,... | collective-permute-start | bytes 24584 | tf_op jit(solution)/shard_map/ppermute | solution.py:15
  14.8 0.9 copy-start.2
  14.8 0.9 copy-start.4
  19.5 0.7 copy-start.5
  19.5 33.1 %copy-start.3 = (f32[4096]{0:T(1024)S(1)}, f32[4096]{0:T(1024)}, u32[]{:S(2)}) copy-start(f32[4096]{0:T(1024)} %param.16) | copy-start | bytes 49156
  19.5 148.0 %all-gather.2.cloned.1.call-start = ((), (), s32[]{:S(2)}) async-start(), calls=%async_computation.5 | async-start | bytes 10485760 | tf_op jit(solution)/shard_map/all_gather | solution.py:118
  167.5 6.5 %copy-start.7 = (bf16[32,32,4096]{2,1,0:T(8,128)(2,1)S(1)}, bf16[32,32,4096]{2,1,0:T(8,128)(2,1)}, u32[]{:S(2)}) copy-start(bf16[32,32,4096]{2,1,0:T(8,128)(2,1)} %all-gather.2.cloned.1.call-done) | copy-start | bytes 25165828
  167.5 7.0 %copy-start.8 = (bf16[1,4096,256]{2,1,0:T(8,128)(2,1)S(1)}, bf16[1,4096,256]{2,1,0:T(8,128)(2,1)}, u32[]{:S(2)}) copy-start(bf16[1,4096,256]{2,1,0:T(8,128)(2,1)} %param.18) | copy-start | bytes 6291460
  283.0 6.2 %copy-start.6 = (f32[256,2]{0,1:T(2,128)S(1)}, f32[256,2]{0,1:T(2,128)}, u32[]{:S(2)}) copy-start(f32[256,2]{0,1:T(2,128)} %param.21) | copy-start | bytes 6148
  283.0 51.6 %all-to-all-start.2 = ((bf16[8,32,4096]{2,1,0:T(8,128)(2,1)}), bf16[8,32,4096]{2,1,0:T(8,128)(2,1)}, u32[]{:S(2)}, u32[]{:S(2)}) async-start(bf16[8,32,4096]{2,1,0:T(8,128)(2,1)} %reduce_sum.44), calls=%async_computation.3 | async-start | bytes 4194304 | tf_op jit(solution)/shard_map/all_to_all | solution.py:125
  347.8 4.9 %copy-start.1 = (bf16[64,4096]{1,0:T(8,128)(2,1)S(1)}, bf16[64,4096]{1,0:T(8,128)(2,1)}, u32[]{:S(2)}) copy-start(bf16[64,4096]{1,0:T(8,128)(2,1)} %reduce-scatter.2.cloned.1.call-done) | copy-start | bytes 1572868
Sparse Core Ops, SparseCore 0:
  19.7 31.4 reduce-scatter.1
  110.7 56.7 all-gather.1
where the time goes:
time: 366 us; the launch traced here: 361 us
  blocking collectives  150 us (41%)
  waiting for transfers between devices  134 us (37%)
  other arithmetic  22.6 us (6%)
  local copies, waits for them, and re-layouts  16.4 us (4%)
  matrix products  15 us (4%)
  between operations  13.7 us (4%)
  starting transfers between devices  9.6 us (3%)
    all_to_all x1, blocking collectives, on_device(): lax.all_to_all(stacked, 'tp', split_axis=0, concat_axis=0, tiled=True)  96.9 us
    all_gather x1, waiting for transfers between devices, on_device(): block_rows = lax.all_gather(arrived, 'tp', axis=0, tiled=True)  56.9 us
    all_to_all x1, blocking collectives, on_device(): lax.all_to_all(outgoing, 'sp', split_axis=0, concat_axis=0, tiled=True)  53.3 us
    all_to_all x1, waiting for transfers between devices, on_device(): lax.all_to_all(summed.astype(jnp.bfloat16), 'sp', split_axis=0, concat_ax...  45.2 us
    reduce_scatter x1, waiting for transfers between devices, on_device(): lax.psum_scatter(rounded(jnp.dot(pooled, out_proj, preferred_element_type...  28.9 us
    gather x2, local copies, waits for them, and re-layouts, collect(): picked = returned[targets]  9.13 us
  transfers between devices with their start and end apart: 4, of which 4 were waited for; matrix products, arithmetic and copies ran while one was open for 1% of the time, Pallas kernels for 0%

commit v1 on v0

--- a/solution.py
+++ b/solution.py
@@ -1,6 +1,10 @@
+import functools
+
 import jax
 import jax.numpy as jnp
 from jax import lax
+from jax.experimental import pallas as pl
+from jax.experimental.pallas import tpu as pltpu
 from jax.sharding import PartitionSpec as P
 
 GROUPS = 4
@@ -52,18 +56,21 @@
 
 def fill_slots(normed, targets, slot_count):
     row_count, width = normed.shape
-    choose = targets.shape[0] // row_count
-    sources = jnp.arange(row_count * choose, dtype=jnp.int32) // choose
-    owner = jnp.full((slot_count,), row_count, jnp.int32).at[targets].set(sources)
-    extended = jnp.concatenate([normed, jnp.zeros((1, width), normed.dtype)], axis=0)
-    return extended[owner]
+    slots = jnp.arange(slot_count, dtype=jnp.int32)[:, None, None]
+    picks = jnp.sum((targets.reshape(row_count, -1)[None] == slots).astype(jnp.bfloat16), axis=2)
+    return jnp.dot(picks, normed, preferred_element_type=jnp.float32).astype(normed.dtype)
 
 
 def collect(returned, targets, weights):
     row_count, choose = weights.shape
-    picked = returned[targets]
-    weighted = picked * weights.reshape(-1, 1)
-    return jnp.sum(weighted.reshape(row_count, choose, -1), axis=1)
+    slots = jnp.arange(returned.shape[0], dtype=jnp.int32)[None, None, :]
+    chosen = targets.reshape(row_count, choose)[:, :, None] == slots
+    spread = jnp.sum(jnp.where(chosen, weights[:, :, None], 0.0), axis=1)
+    head = lax.reduce_precision(spread, 8, 7)
+    tail = spread - head
+    both = jnp.concatenate([head, tail], axis=0).astype(jnp.bfloat16)
+    product = jnp.dot(both, returned, preferred_element_type=jnp.float32)
+    return product[:row_count] + product[row_count:]
 
 
 def expert_part(inputs, w_gate, w_up, w_down):
@@ -71,6 +78,239 @@
     upper = jnp.dot(inputs, w_up[0], preferred_element_type=jnp.float32)
     hidden = (jax.nn.silu(gate) * upper).astype(jnp.bfloat16)
     return jnp.dot(hidden, w_down[0], preferred_element_type=jnp.float32).astype(jnp.bfloat16)
+
+
+def xor_of(a, b, n):
+    total, bit = 0, 1
+    while bit < n:
+        total = total + ((a // bit + b // bit) % 2) * bit
+        bit *= 2
+    return total
+
+
+def moe_kernel(
+    n, slices, capacity,
+    outgoing, wg_hbm, wu_hbm, wd_hbm, out,
+    wg, wu, wd, rows, parts, pair_in, y_in,
+    w_sem, own_sem,
+    sp_send, sp_recv, fy_send, fy_recv, fa_send, fa_recv, fb_send, fb_recv,
+    pp_send, pp_recv, ry_send, ry_recv, rs_send, rs_recv,
+):
+    me = lax.axis_index("sp")
+    tp = lax.axis_index("tp")
+    core, y = tp % 2, tp // 2
+    mate = y * 2 + (1 - core)
+    across = (1 - y) * 2 + core
+    C = capacity
+
+    def spot(c, yy):
+        return pl.ds(pl.multiple_of((c * 2 + yy) * C, C), C)
+
+    def half(c):
+        return pl.ds(pl.multiple_of(c * 2 * C, 2 * C), 2 * C)
+
+    def offset(j):
+        return jnp.where(j < 2, j, n + 1 - j)
+
+    def chunk(j):
+        return xor_of(me, offset(j), n)
+
+    def remote(src, dst, send, recv, to):
+        return pltpu.make_async_remote_copy(
+            src_ref=src, dst_ref=dst, send_sem=send, recv_sem=recv,
+            device_id=to, device_id_type=pl.DeviceIdType.MESH,
+        )
+
+    def sp_copy(j):
+        s = chunk(j)
+        return remote(outgoing.at[s], rows.at[me, spot(core, y)],
+                      sp_send.at[j], sp_recv.at[j], (s, tp))
+
+    def fy_copy(j):
+        s = chunk(j)
+        ref = rows.at[s, spot(core, y)]
+        return remote(ref, ref, fy_send.at[j], fy_recv.at[j], (me, across))
+
+    def fa_copy(j):
+        s = chunk(j)
+        ref = rows.at[s, spot(core, y)]
+        return remote(ref, ref, fa_send.at[j], fa_recv.at[j], (me, mate))
+
+    def fb_copy(j):
+        s = chunk(j)
+        ref = rows.at[s, spot(core, 1 - y)]
+        return remote(ref, ref, fb_send.at[j], fb_recv.at[j], (me, mate))
+
+    def pp_copy(j):
+        s = chunk(j)
+        return remote(parts.at[s, half(1 - core)], pair_in.at[s],
+                      pp_send.at[j], pp_recv.at[j], (me, mate))
+
+    def ry_copy(j):
+        s = chunk(j)
+        return remote(parts.at[s, spot(core, 1 - y)], y_in.at[s],
+                      ry_send.at[j], ry_recv.at[j], (me, across))
+
+    def rs_copy(j):
+        s = chunk(j)
+        return remote(parts.at[s, spot(core, y)], out.at[me],
+                      rs_send.at[j], rs_recv.at[j], (s, tp))
+
+    loads = [
+        pltpu.make_async_copy(wg_hbm.at[0], wg, w_sem.at[0]),
+        pltpu.make_async_copy(wu_hbm.at[0], wu, w_sem.at[1]),
+        pltpu.make_async_copy(wd_hbm.at[0], wd, w_sem.at[2]),
+    ]
+    own = pltpu.make_async_copy(outgoing.at[me], rows.at[me, spot(core, y)], own_sem)
+    own.start()
+
+    barrier = pltpu.get_barrier_semaphore()
+
+    @pl.loop(1, n)
+    def _(j):
+        pl.semaphore_signal(barrier, inc=1, device_id=(xor_of(me, j, n), tp),
+                               device_id_type=pl.DeviceIdType.MESH)
+
+    for peer in (mate, across):
+        pl.semaphore_signal(barrier, inc=1, device_id=(me, peer),
+                               device_id_type=pl.DeviceIdType.MESH)
+    pl.semaphore_wait(barrier, n + 1)
+
+    @pl.loop(1, n)
+    def _(j):
+        sp_copy(j).start()
+
+    for load in loads:
+        load.start()
+
+    def compute(s):
+        x = rows[s]
+        gate = jnp.dot(x, wg[...], preferred_element_type=jnp.float32)
+        upper = jnp.dot(x, wu[...], preferred_element_type=jnp.float32)
+        hidden = (gate * (1.0 / (1.0 + jnp.exp(-gate))) * upper).astype(jnp.bfloat16)
+        width = wd.shape[1]
+        tile = min(1024, width)
+
+        @pl.loop(0, width // tile)
+        def _(k):
+            cols = pl.ds(pl.multiple_of(k * tile, tile), tile)
+            parts[s, :, cols] = jnp.dot(
+                hidden, wd[:, cols], preferred_element_type=jnp.float32
+            ).astype(jnp.bfloat16)
+
+    @pl.loop(0, n + 3)
+    def _(j):
+        @pl.when(j == 0)
+        def _():
+            own.wait()
+
+        @pl.when((j >= 1) & (j < n))
+        def _():
+            sp_copy(j).wait_recv()
+
+        @pl.when(j < n)
+        def _():
+            fy_copy(j).start()
+            fa_copy(j).start()
+
+        @pl.when((j >= 2) & (j < n + 2))
+        def _():
+            k = j - 2
+            s = chunk(k)
+            pp_copy(k).wait_recv()
+            there = spot(core, 1 - y)
+            far = pl.ds(pl.multiple_of((1 - y) * C, C), C)
+            parts[s, there] = (
+                parts[s, there].astype(jnp.float32) + pair_in[s, far].astype(jnp.float32)
+            ).astype(jnp.bfloat16)
+            ry_copy(k).start()
+
+        @pl.when(j >= 3)
+        def _():
+            k = j - 3
+            s = chunk(k)
+            ry_copy(k).wait_recv()
+            here = spot(core, y)
+            near = pl.ds(pl.multiple_of(y * C, C), C)
+            total = (
+                parts[s, here].astype(jnp.float32)
+                + pair_in[s, near].astype(jnp.float32)
+                + y_in[s].astype(jnp.float32)
+            ).astype(jnp.bfloat16)
+
+            @pl.when(k == 0)
+            def _():
+                out[me] = total
+
+            @pl.when(k > 0)
+            def _():
+                parts[s, here] = total
+                rs_copy(k).start()
+
+        @pl.when((j >= 1) & (j < n + 1))
+        def _():
+            k = j - 1
+            fy_copy(k).wait_recv()
+            fb_copy(k).start()
+
+            @pl.when(k == 0)
+            def _():
+                for load in loads:
+                    load.wait()
+
+            fa_copy(k).wait_recv()
+            fb_copy(k).wait_recv()
+            compute(chunk(k))
+            pp_copy(k).start()
+
+    @pl.loop(0, n)
+    def _(j):
+        fy_copy(j).wait_send()
+        fa_copy(j).wait_send()
+        fb_copy(j).wait_send()
+        pp_copy(j).wait_send()
+        ry_copy(j).wait_send()
+
+        @pl.when(j > 0)
+        def _():
+            sp_copy(j).wait_send()
+            rs_copy(j).wait_send()
+            rs_copy(j).wait_recv()
+
+
+def moe_exchange(outgoing, w_gate, w_up, w_down, slices):
+    n, capacity, width = outgoing.shape
+    units = w_gate.shape[2]
+    bf16 = jnp.bfloat16
+    dma = pltpu.SemaphoreType.DMA
+    return pl.pallas_call(
+        functools.partial(moe_kernel, n, slices, capacity),
+        out_shape=jax.ShapeDtypeStruct(outgoing.shape, bf16),
+        in_specs=[pl.BlockSpec(memory_space=pltpu.VMEM)]
+        + [pl.BlockSpec(memory_space=pl.ANY)] * 3,
+        out_specs=pl.BlockSpec(memory_space=pltpu.VMEM),
+        scratch_shapes=[
+            pltpu.VMEM((width, units), bf16),
+            pltpu.VMEM((width, units), bf16),
+            pltpu.VMEM((units, width), bf16),
+            pltpu.VMEM((n, slices * capacity, width), bf16),
+            pltpu.VMEM((n, slices * capacity, width), bf16),
+            pltpu.VMEM((n, 2 * capacity, width), bf16),
+            pltpu.VMEM((n, capacity, width), bf16),
+            dma((3,)),
+            dma,
+        ]
+        + [dma((n,))] * 14,
+        compiler_params=pltpu.CompilerParams(
+            collective_id=1, has_side_effects=True, vmem_limit_bytes=52 * 2**20
+        ),
+        cost_estimate=pl.CostEstimate(
+            flops=6 * n * slices * capacity * width * units,
+            bytes_accessed=3 * 2 * width * units,
+            transcendentals=0,
+        ),
+        name="moe_exchange",
+    )(outgoing, w_gate, w_up, w_down)
 
 
 def on_device(
@@ -114,17 +354,20 @@
     weight_rows = lax.dynamic_slice_in_dim(route_weight, first, sub_count, 0)
     targets = slot_plan(route_rows, 1, capacity, experts)
     outgoing = fill_slots(normed, targets, experts * capacity).reshape(experts, capacity, width)
-    arrived = lax.all_to_all(outgoing, "sp", split_axis=0, concat_axis=0, tiled=True)
-    block_rows = lax.all_gather(arrived, "tp", axis=0, tiled=True)
-    spread = expert_part(block_rows.reshape(-1, width), w_gate, w_up, w_down).reshape(
-        block_rows.shape
-    )
-    stacked = spread.reshape((slices,) + arrived.shape)
-    received = lax.all_to_all(stacked, "tp", split_axis=0, concat_axis=0, tiled=True)
-    summed = jnp.sum(received.astype(jnp.float32), axis=0)
-    returned = lax.all_to_all(
-        summed.astype(jnp.bfloat16), "sp", split_axis=0, concat_axis=0, tiled=True
-    ).astype(summed.dtype)
+    if slices == 4 and capacity % 16 == 0 and experts & (experts - 1) == 0:
+        returned = moe_exchange(outgoing, w_gate, w_up, w_down, slices)
+    else:
+        arrived = lax.all_to_all(outgoing, "sp", split_axis=0, concat_axis=0, tiled=True)
+        block_rows = lax.all_gather(arrived, "tp", axis=0, tiled=True)
+        spread = expert_part(block_rows.reshape(-1, width), w_gate, w_up, w_down).reshape(
+            block_rows.shape
+        )
+        stacked = spread.reshape((slices,) + arrived.shape)
+        received = lax.all_to_all(stacked, "tp", split_axis=0, concat_axis=0, tiled=True)
+        summed = jnp.sum(received.astype(jnp.float32), axis=0)
+        returned = lax.all_to_all(
+            summed.astype(jnp.bfloat16), "sp", split_axis=0, concat_axis=0, tiled=True
+        )
     moe = collect(returned.reshape(-1, width), targets, weight_rows)
     return (mixed + moe).astype(jnp.bfloat16)
 

time: 366 us -> 195 us (0.53)
  blocking collectives: 150 us -> 0 us
  Pallas kernels: 0 us -> 126 us
  waiting for transfers between devices: 134 us -> 32.6 us
  other arithmetic: 22.6 us -> 5.61 us
  local copies, waits for them, and re-layouts: 16.4 us -> 2.54 us
  matrix products: 15 us -> 7.65 us
  starting transfers between devices: 9.6 us -> 3.39 us
    all_to_all x2 -> x0, blocking collectives: 150 us -> none  [the longest x1 96.9 us: on_device(): lax.all_to_all(stacked, 'tp', split_axis=0, concat_axis=0, tiled=True)]
    pallas_call x0 -> x1, Pallas kernels: none -> 126 us  [moe_exchange(): pl.pallas_call(functools.partial(moe_kernel, n, slices, capacity), out_sh...]
    all_gather x1 -> x0, waiting for transfers between devices: 56.9 us -> none  [on_device(): block_rows = lax.all_gather(arrived, 'tp', axis=0, tiled=True)]
    all_to_all x1 -> x0, waiting for transfers between devices: 45.2 us -> none  [on_device(): lax.all_to_all(summed.astype(jnp.bfloat16), 'sp', split_axis=0, concat_ax...]
    gather x3 -> x0, local copies, waits for them, and re-layouts: 12.3 us -> none  [the longest x2 9.13 us: collect(): picked = returned[targets]]
    reduce_sum x2, other arithmetic: 11.8 us -> 0.2 us  [the longest x1 0.1 us: collect(): spread = jnp.sum(jnp.where(chosen, weights[:, :, None], 0.0), axis=1)]
    all_to_all x1 -> x0, starting transfers between devices: 6.17 us -> none  [on_device(): lax.all_to_all(summed.astype(jnp.bfloat16), 'sp', split_axis=0, concat_ax...]
    dot_general x3 -> x2, matrix products: 11.2 us -> 5.42 us  [the longest x1 3.32 us: fill_slots(): jnp.dot(picks, normed, preferred_element_type=jnp.float32)]
  transfers between devices with their start and end apart: 4 -> 2, of which waited for: 4 -> 2; matrix products, arithmetic and copies ran while one was open for 1% -> 1% of each run, Pallas kernels for 0% -> 0%
where the time goes in v1:
time: 195 us; the launch traced here: 191 us
  Pallas kernels  126 us (65%)
  waiting for transfers between devices  32.6 us (17%)
  between operations  13.6 us (7%)
  matrix products  7.65 us (4%)
  other arithmetic  5.61 us (3%)
  starting transfers between devices  3.39 us (2%)
  local copies, waits for them, and re-layouts  2.54 us (1%)
    pallas_call x1, Pallas kernels, moe_exchange(): pl.pallas_call(functools.partial(moe_kernel, n, slices, capacity), out_sh...  126 us
    reduce_scatter x1, waiting for transfers between devices, on_device(): lax.psum_scatter(rounded(jnp.dot(pooled, out_proj, preferred_element_type...  29.6 us
  transfers between devices with their start and end apart: 2, of which 2 were waited for; matrix products, arithmetic and copies ran while one was open for 1% of the time, Pallas kernels for 0%

profile of v1, /device:TPU:8, one launch (start us, length us, event | category | flops | bytes accessed | tf_op | source)
XLA Modules:
  0.0 191.3 jit_solution(13889681108636648165)
XLA Ops:
  6.5 0.0 copy-start
  6.5 0.0 reduce-scatter.2.cloned.1.call-start
  6.5 0.8 slice.25
  7.4 3.4 %collective-permute-start = (bf16[16,256]{1,0:T(8,128)(2,1)S(1)}, bf16[16,256]{1,0:T(8,128)(2,1)S(1)}, u32[]{:S(2)}, u32[]{:S(2)}) collective-permute-start(bf16[16,256]{1,0:T(8,128)(2,1)S(1)} %slice.25), channel_id=1, source_target_pairs={{0,4},{4,8},{8,12},{12,16},{16,20},{20,24},{24,28},{1,5},{5,9},{9,... | collective-permute-start | bytes 24584 | tf_op jit(solution)/shard_map/ppermute | solution.py:19
  10.8 3.0 %collective-permute-done = bf16[16,256]{1,0:T(8,128)(2,1)S(1)} collective-permute-done((bf16[16,256]{1,0:T(8,128)(2,1)S(1)}, bf16[16,256]{1,0:T(8,128)(2,1)S(1)}, u32[]{:S(2)}, u32[]{:S(2)}) %collective-permute-start) | collective-permute-done | bytes 8224 | tf_op jit(solution)/shard_map/ppermute | solution.py:19
  13.8 0.9 fusion.25
  14.8 0.0 copy-start.2
  14.8 0.0 copy-start.5
  14.8 0.3 fusion.3
  15.2 0.1 broadcast_add_fusion
  15.3 0.1 copy.25
  15.4 0.0 copy-done
  15.4 0.3 copy-done.2
  15.7 0.0 copy-done.5
  15.7 2.2 %convolution_convert_fusion.1 = bf16[256,4096]{1,0:T(8,128)(2,1)} fusion(bf16[256,4096]{1,0:T(8,128)(2,1)S(1)} %copy-done, f32[272,256]{1,0:T(8,128)S(1)} %get-tuple-element.6, f32[384,256]{1,0:T(8,128)S(1)} %bitcast.19, f32[272,256]{1,0:T(8,128)S(1)} %slice.36, s32[]{:T(128)S(6)} %select_n.13, bf16[1,256,256]{2,1,0:T(8,128)(2,1)S(1)} %copy-done.2, ...), kind=kOutput, calls=%fused_computation.1 | convolution fusion | flops 571867136 | bytes 5113860 | tf_op jit(solution)/shard_map/dot_general | solution.py:342
  17.9 0.0 copy-start.4
  17.9 0.0 copy-start.6
  17.9 0.0 copy-start.3
  17.9 0.0 reduce-scatter.2.cloned.1.call-update
  17.9 0.6 copy-done.4
  18.6 0.1 constant_dynamic-slice_fusion.1
  18.7 0.1 copy.26
  18.8 0.1 eq.53
  18.9 0.1 fusion.24
  19.0 0.2 reduce_window_sum.28
  19.2 0.2 select_reduce_fusion.1
  19.3 0.1 reduce_sum.42
  19.5 0.1 copy.27
  19.6 0.0 copy-done.6
  19.6 0.1 constant_dynamic-slice_fusion
  19.7 0.1 multiply_add_fusion
  19.7 0.1 fusion.19
  19.8 0.1 select_reduce_fusion
  20.0 29.6 %reduce-scatter.2.cloned.1.call-done = bf16[64,4096]{1,0:T(8,128)(2,1)} async-done(((bf16[256,4096]{1,0:T(8,128)(2,1)}), bf16[64,4096]{1,0:T(8,128)(2,1)}) %reduce-scatter.2.cloned.1.call-update) | async-done | bytes 524304 | tf_op jit(solution)/shard_map/reduce_scatter | solution.py:341
  49.6 1.5 multiply_reduce_fusion
  51.0 0.0 copy-done.3
  51.1 3.3 %convolution_convert_fusion = bf16[256,4096]{1,0:T(8,128)(2,1)} fusion(bf16[256,64]{0,1:T(8,128)(2,1)S(1)} %fusion.19, bf16[64,4096]{1,0:T(8,128)(2,1)} %reduce-scatter.2.cloned.1.call-done, f32[4096]{0:T(1024)S(1)} %copy-done.3, f32[64]{0:T(128)S(1)} %add_rsqrt_fusion, bf16[256,4096]{1,0:T(8,128)(2,1)} %param.11, s32[]{:T(128)S(6)} %select_n.12), kind=kOutput, calls=%fused_computation | convolution fusion | flops 136839168 | bytes 3195140 | tf_op jit(solution)/shard_map/dot_general | solution.py:61
  54.4 125.9 %moe_exchange.1 = bf16[8,32,4096]{2,1,0:T(8,128)(2,1)} custom-call(bf16[8,32,4096]{2,1,0:T(8,128)(2,1)} %bitcast.21, bf16[1,4096,256]{2,1,0:T(8,128)(2,1)} %wg_hbm.1, bf16[1,4096,256]{2,1,0:T(8,128)(2,1)} %wu_hbm.1, bf16[1,256,4096]{2,1,0:T(8,128)(2,1)} %wd_hbm.1), custom_call_target="tpu_custom_call" | custom-call | flops 6442450944 | bytes 6291456 | tf_op jit(solution)/shard_map/moe_exchange/pallas_call | solution.py:286
  180.3 0.0 copy-start.1
  180.3 2.1 %fusion.20 = f32[128,4096]{1,0:T(8,128)S(1)} fusion(bf16[256,4096]{1,0:T(8,128)(2,1)} %bitcast.20, bf16[64,256]{1,0:T(8,128)(2,1)S(1)} %get-tuple-element.8, bf16[64,256]{1,0:T(8,128)(2,1)S(1)} %get-tuple-element.7), kind=kOutput, calls=%fused_computation.32 | convolution fusion | flops 268566528 | bytes 4259840 | tf_op jit(solution)/shard_map/dot_general | solution.py:72
  182.4 0.0 copy-done.1
  182.4 2.1 %fusion.2 = bf16[64,4096]{1,0:T(8,128)(2,1)} fusion(f32[128,4096]{1,0:T(8,128)S(1)} %fusion.20, bf16[64,4096]{1,0:T(8,128)(2,1)S(1)} %copy-done.1, bf16[256,4096]{1,0:T(8,128)(2,1)} %param.11, s32[]{:T(128)S(6)} %select_n.12), kind=kLoop, calls=%fused_computation.6 | loop fusion | flops 1572864 | bytes 3670020 | tf_op jit(solution)/shard_map/convert_element_type | solution.py:372
  (7 shorter events, 0.1 us)
Async XLA Ops:
  6.5 8.8 %copy-start = (bf16[256,4096]{1,0:T(8,128)(2,1)S(1)}, bf16[256,4096]{1,0:T(8,128)(2,1)}, u32[]{:S(2)}) copy-start(bf16[256,4096]{1,0:T(8,128)(2,1)} %param.15) | copy-start | bytes 6291460
  6.5 43.0 %reduce-scatter.2.cloned.1.call-start = ((), (), s32[]{:S(2)}) async-start(), calls=%async_computation.1 | async-start | bytes 2621440 | tf_op jit(solution)/shard_map/reduce_scatter | solution.py:341
  7.4 6.4 %collective-permute-start = (bf16[16,256]{1,0:T(8,128)(2,1)S(1)}, bf16[16,256]{1,0:T(8,128)(2,1)S(1)}, u32[]{:S(2)}, u32[]{:S(2)}) collective-permute-start(bf16[16,256]{1,0:T(8,128)(2,1)S(1)} %slice.25), channel_id=1, source_target_pairs={{0,4},{4,8},{8,12},{12,16},{16,20},{20,24},{24,28},{1,5},{5,9},{9,... | collective-permute-start | bytes 24584 | tf_op jit(solution)/shard_map/ppermute | solution.py:19
  14.8 0.9 copy-start.2
  14.8 0.9 copy-start.5
  17.9 0.7 copy-start.4
  17.9 1.7 copy-start.6
  17.9 33.1 %copy-start.3 = (f32[4096]{0:T(1024)S(1)}, f32[4096]{0:T(1024)}, u32[]{:S(2)}) copy-start(f32[4096]{0:T(1024)} %param.16) | copy-start | bytes 49156
  180.3 2.1 %copy-start.1 = (bf16[64,4096]{1,0:T(8,128)(2,1)S(1)}, bf16[64,4096]{1,0:T(8,128)(2,1)}, u32[]{:S(2)}) copy-start(bf16[64,4096]{1,0:T(8,128)(2,1)} %reduce-scatter.2.cloned.1.call-done) | copy-start | bytes 1572868
Sparse Core Ops, SparseCore 0:
  18.1 31.4 reduce-scatter.1

commit v2 on v1

--- a/solution.py
+++ b/solution.py
@@ -110,7 +110,7 @@
         return pl.ds(pl.multiple_of(c * 2 * C, 2 * C), 2 * C)
 
     def offset(j):
-        return jnp.where(j < 2, j, n + 1 - j)
+        return j
 
     def chunk(j):
         return xor_of(me, offset(j), n)
@@ -313,6 +313,101 @@
     )(outgoing, w_gate, w_up, w_down)
 
 
+def sum_kernel(count, part, out, pair_in, total, y_in, pp_send, pp_recv, y_send, y_recv):
+    me = lax.axis_index("sp")
+    tp = lax.axis_index("tp")
+    core, y = tp % 2, tp // 2
+    mate = y * 2 + (1 - core)
+    across = (1 - y) * 2 + core
+    pieces = count // 16
+    mesh_id = pl.DeviceIdType.MESH
+    barrier = pltpu.get_barrier_semaphore()
+    for peer in (mate, across):
+        pl.semaphore_signal(barrier, inc=1, device_id=(me, peer), device_id_type=mesh_id)
+    pl.semaphore_wait(barrier, 2)
+
+    def at(yy, c, k):
+        return pl.ds(pl.multiple_of((yy * 2 + c) * count + k * 16, 16), 16)
+
+    def piece(k):
+        return pl.ds(pl.multiple_of(k * 16, 16), 16)
+
+    def pair_copy(yy, k, place):
+        return pltpu.make_async_remote_copy(
+            src_ref=part.at[at(yy, 1 - core, k)], dst_ref=pair_in.at[place, piece(k)],
+            send_sem=pp_send.at[place, k], recv_sem=pp_recv.at[place, k],
+            device_id=(me, mate), device_id_type=mesh_id,
+        )
+
+    def far_copy(k):
+        return pltpu.make_async_remote_copy(
+            src_ref=total.at[piece(k)], dst_ref=y_in.at[piece(k)],
+            send_sem=y_send.at[k], recv_sem=y_recv.at[k],
+            device_id=(me, across), device_id_type=mesh_id,
+        )
+
+    @pl.loop(0, pieces)
+    def _(k):
+        pair_copy(1 - y, k, 0).start()
+
+    @pl.loop(0, pieces)
+    def _(k):
+        pair_copy(y, k, 1).start()
+
+    @pl.loop(0, pieces)
+    def _(k):
+        pair_copy(1 - y, k, 0).wait_recv()
+        total[piece(k)] = (
+            part[at(1 - y, core, k)].astype(jnp.float32)
+            + pair_in[0, piece(k)].astype(jnp.float32)
+        ).astype(jnp.bfloat16)
+        far_copy(k).start()
+
+    @pl.loop(0, pieces)
+    def _(k):
+        pair_copy(y, k, 1).wait_recv()
+        far_copy(k).wait_recv()
+        out[piece(k)] = (
+            part[at(y, core, k)].astype(jnp.float32)
+            + pair_in[1, piece(k)].astype(jnp.float32)
+            + y_in[piece(k)].astype(jnp.float32)
+        ).astype(jnp.bfloat16)
+
+    @pl.loop(0, pieces)
+    def _(k):
+        pair_copy(1 - y, k, 0).wait_send()
+        pair_copy(y, k, 1).wait_send()
+        far_copy(k).wait_send()
+
+
+def scatter_sum(part, slices):
+    row_count, width = part.shape
+    count = row_count // slices
+    pieces = count // 16
+    bf16 = jnp.bfloat16
+    dma = pltpu.SemaphoreType.DMA
+    return pl.pallas_call(
+        functools.partial(sum_kernel, count),
+        out_shape=jax.ShapeDtypeStruct((count, width), bf16),
+        in_specs=[pl.BlockSpec(memory_space=pltpu.VMEM)],
+        out_specs=pl.BlockSpec(memory_space=pltpu.VMEM),
+        scratch_shapes=[
+            pltpu.VMEM((2, count, width), bf16),
+            pltpu.VMEM((count, width), bf16),
+            pltpu.VMEM((count, width), bf16),
+            dma((2, pieces)),
+            dma((2, pieces)),
+            dma((pieces,)),
+            dma((pieces,)),
+        ],
+        compiler_params=pltpu.CompilerParams(
+            collective_id=2, has_side_effects=True, vmem_limit_bytes=24 * 2**20
+        ),
+        cost_estimate=pl.CostEstimate(flops=0, bytes_accessed=2**25, transcendentals=0),
+        name="scatter_sum",
+    )(part)
+
+
 def on_device(
     resid,
     pool_in,
@@ -337,16 +432,15 @@
     pooled = (jnp.dot(diff, pool_mix[0], preferred_element_type=jnp.float32) * pool_gain).astype(
         jnp.bfloat16
     )
-    proj = rounded(
-        lax.psum_scatter(
-            rounded(jnp.dot(pooled, out_proj, preferred_element_type=jnp.float32)).astype(
-                jnp.bfloat16
-            ),
-            "tp",
-            scatter_dimension=0,
-            tiled=True,
-        ).astype(jnp.float32)
+    group_part = rounded(jnp.dot(pooled, out_proj, preferred_element_type=jnp.float32)).astype(
+        jnp.bfloat16
     )
+    if slices == 4 and sub_count % 16 == 0:
+        proj = scatter_sum(group_part, slices).astype(jnp.float32)
+    else:
+        proj = rounded(
+            lax.psum_scatter(group_part, "tp", scatter_dimension=0, tiled=True).astype(jnp.float32)
+        )
     first = tp_index * sub_count
     mixed = lax.dynamic_slice_in_dim(resid, first, sub_count, 0).astype(jnp.float32) + proj
     normed = normalize(mixed, norm_gain)

time: 195 us -> 160 us (0.82); the launches traced: 191 us -> 159 us
  waiting for transfers between devices: 32.6 us -> 0.01 us
  Pallas kernels: 126 us -> 140 us
  between operations: 13.6 us -> 0.2 us
  local copies, waits for them, and re-layouts: 2.54 us -> 4.84 us
    reduce_scatter x1 -> x0, waiting for transfers between devices: 29.6 us -> none  [on_device(): lax.psum_scatter(rounded(jnp.dot(pooled, out_proj, preferred_element_type...]
    pallas_call x0 -> x1, Pallas kernels: none -> 15.8 us  [scatter_sum(): pl.pallas_call(functools.partial(sum_kernel, count), out_shape=jax.ShapeD...]
    ppermute x1, waiting for transfers between devices: 3.01 us -> 0.01 us  [shifted(): return lax.ppermute(x, axis, pairs)]
  transfers between devices with their start and end apart: 2 -> 1, of which waited for: 2 -> 0; matrix products, arithmetic and copies ran while one was open for 1% -> 2% of each run, Pallas kernels for 0% -> 0%
where the time goes in v2:
time: 160 us; the launch traced here: 159 us
  Pallas kernels  140 us (88%)
  matrix products  6.4 us (4%)
  local copies, waits for them, and re-layouts  4.84 us (3%)
  other arithmetic  4.03 us (3%)
  starting transfers between devices  3.39 us (2%)
    pallas_call x1, Pallas kernels, moe_exchange(): pl.pallas_call(functools.partial(moe_kernel, n, slices, capacity), out_sh...  125 us
    pallas_call x1, Pallas kernels, scatter_sum(): pl.pallas_call(functools.partial(sum_kernel, count), out_shape=jax.ShapeD...  15.8 us
    ppermute x1, starting transfers between devices, shifted(): return lax.ppermute(x, axis, pairs)  3.39 us
  transfers between devices with their start and end apart: 1, of which 0 were waited for; matrix products, arithmetic and copies ran while one was open for 2% of the time, Pallas kernels for 0%

profile of v2, /device:TPU:8, one launch (start us, length us, event | category | flops | bytes accessed | tf_op | source)
XLA Modules:
  0.0 159.2 jit_solution(12985339035720144108)
XLA Ops:
  0.0 0.0 copy-start
  0.0 0.8 slice.25
  0.9 3.4 %collective-permute-start = (bf16[16,256]{1,0:T(8,128)(2,1)S(1)}, bf16[16,256]{1,0:T(8,128)(2,1)S(1)}, u32[]{:S(2)}, u32[]{:S(2)}) collective-permute-start(bf16[16,256]{1,0:T(8,128)(2,1)S(1)} %slice.25), channel_id=1, source_target_pairs={{0,4},{4,8},{8,12},{12,16},{16,20},{20,24},{24,28},{1,5},{5,9},{9,... | collective-permute-start | bytes 24584 | tf_op jit(solution)/shard_map/ppermute | solution.py:19
  4.3 0.8 constant_dynamic-slice_fusion
  5.0 0.7 constant_dynamic-slice_fusion.1
  5.8 0.1 copy.26
  5.9 0.1 eq.53
  6.0 0.1 fusion.24
  6.1 0.2 reduce_window_sum.28
  6.3 0.2 select_reduce_fusion.1
  6.4 0.1 reduce_sum.42
  6.6 0.1 copy.27
  6.7 0.8 multiply_add_fusion
  7.4 0.1 fusion.19
  7.5 0.1 select_reduce_fusion
  7.7 0.0 collective-permute-done
  7.7 0.9 fusion.25
  8.6 0.0 copy-start.3
  8.6 0.0 copy-start.5
  8.7 0.3 fusion.3
  9.0 0.1 broadcast_add_fusion
  9.1 0.1 copy.25
  9.2 0.0 copy-done
  9.2 0.3 copy-done.3
  9.5 0.0 copy-done.5
  9.5 2.2 %convolution_convert_fusion.1.part = bf16[256,4096]{1,0:T(8,128)(2,1)} fusion(bf16[256,4096]{1,0:T(8,128)(2,1)S(1)} %copy-done, f32[272,256]{1,0:T(8,128)S(1)} %get-tuple-element.6, f32[384,256]{1,0:T(8,128)S(1)} %bitcast.19, f32[272,256]{1,0:T(8,128)S(1)} %slice.36, s32[]{:T(128)S(6)} %select_n.13, bf16[1,256,256]{2,1,0:T(8,128)(2,1)S(1)} %copy-done.3, ...), kind=kOutput, calls=%fused_computation.1 | convolution fusion | flops 571867136 | bytes 5113860 | tf_op jit(solution)/shard_map/dot_general | solution.py:435
  11.8 0.0 copy-start.1
  11.8 1.6 copy-done.1
  13.4 0.0 copy-start.2
  13.4 0.0 copy-start.4
  13.4 15.8 %scatter_sum.1 = bf16[64,4096]{1,0:T(8,128)(2,1)S(1)} custom-call(bf16[256,4096]{1,0:T(8,128)(2,1)S(1)} %copy-done.1), custom_call_target="tpu_custom_call" | custom-call | bytes 33554432 | tf_op jit(solution)/shard_map/scatter_sum/pallas_call | solution.py:389
  29.2 0.0 copy-done.2
  29.2 0.3 multiply_reduce_fusion
  29.5 0.0 copy-done.4
  29.5 2.1 %convolution_convert_fusion = bf16[256,4096]{1,0:T(8,128)(2,1)} fusion(bf16[256,64]{0,1:T(8,128)(2,1)S(1)} %fusion.19, bf16[64,4096]{1,0:T(8,128)(2,1)S(1)} %scatter_sum.1, f32[4096]{0:T(1024)S(1)} %copy-done.4, f32[64]{0:T(128)S(1)} %add_rsqrt_fusion, bf16[256,4096]{1,0:T(8,128)(2,1)S(1)} %copy-done.2, s32[]{:T(128)S(6)} %select_n.12), kind=kOutput, calls=%fused_computation | convolution fusion | flops 136839168 | bytes 3195396 | tf_op jit(solution)/shard_map/dot_general | solution.py:61
  31.6 124.6 %moe_exchange.1 = bf16[8,32,4096]{2,1,0:T(8,128)(2,1)} custom-call(bf16[8,32,4096]{2,1,0:T(8,128)(2,1)} %bitcast.21, bf16[1,4096,256]{2,1,0:T(8,128)(2,1)} %wg_hbm.1, bf16[1,4096,256]{2,1,0:T(8,128)(2,1)} %wu_hbm.1, bf16[1,256,4096]{2,1,0:T(8,128)(2,1)} %wd_hbm.1), custom_call_target="tpu_custom_call" | custom-call | flops 6442450944 | bytes 6291456 | tf_op jit(solution)/shard_map/moe_exchange/pallas_call | solution.py:286
  156.2 2.0 %fusion.20 = f32[128,4096]{1,0:T(8,128)S(1)} fusion(bf16[256,4096]{1,0:T(8,128)(2,1)} %bitcast.20, bf16[64,256]{1,0:T(8,128)(2,1)S(1)} %get-tuple-element.8, bf16[64,256]{1,0:T(8,128)(2,1)S(1)} %get-tuple-element.7), kind=kOutput, calls=%fused_computation.32 | convolution fusion | flops 268566528 | bytes 4259840 | tf_op jit(solution)/shard_map/dot_general | solution.py:72
  158.2 1.0 fusion.2
  (7 shorter events, 0.1 us)
Async XLA Ops:
  0.0 9.2 %copy-start = (bf16[256,4096]{1,0:T(8,128)(2,1)S(1)}, bf16[256,4096]{1,0:T(8,128)(2,1)}, u32[]{:S(2)}) copy-start(bf16[256,4096]{1,0:T(8,128)(2,1)} %param.15) | copy-start | bytes 6291460
  0.9 6.8 %collective-permute-start = (bf16[16,256]{1,0:T(8,128)(2,1)S(1)}, bf16[16,256]{1,0:T(8,128)(2,1)S(1)}, u32[]{:S(2)}, u32[]{:S(2)}) collective-permute-start(bf16[16,256]{1,0:T(8,128)(2,1)S(1)} %slice.25), channel_id=1, source_target_pairs={{0,4},{4,8},{8,12},{12,16},{16,20},{20,24},{24,28},{1,5},{5,9},{9,... | collective-permute-start | bytes 24584 | tf_op jit(solution)/shard_map/ppermute | solution.py:19
  8.6 0.9 copy-start.3
  8.6 0.9 copy-start.5
  11.8 1.6 copy-start.1
  13.4 15.8 %copy-start.2 = (bf16[256,4096]{1,0:T(8,128)(2,1)S(1)}, bf16[256,4096]{1,0:T(8,128)(2,1)}, u32[]{:S(2)}) copy-start(bf16[256,4096]{1,0:T(8,128)(2,1)} %param.11) | copy-start | bytes 6291460
  13.4 16.1 %copy-start.4 = (f32[4096]{0:T(1024)S(1)}, f32[4096]{0:T(1024)}, u32[]{:S(2)}) copy-start(f32[4096]{0:T(1024)} %param.16) | copy-start | bytes 49156
